TPU v7x, 32 devices: a whole 2x2x4 slice. The times are simulated.
32 devices in a mesh: grp: 2 (over y), sp: 4 (over z), tp: 4 (over x, core).
Axes of the slice: x: 2, y: 2, z: 4, core: 2. Of those that a mesh axis runs over, the one named last changes fastest.
Arguments:
- target: bfloat16 [1024, 2048], P(('grp', 'sp', 'tp')), parts along dimension 0, may hold values from -6 to 6
- source: bfloat16 [8192, 2048], P(('grp', 'sp', 'tp')), parts along dimension 0, may hold values from -6 to 6
- norm_gain: float32 [2048], replicated, may hold values from 0.1 to 1.9
- query_weight: bfloat16 [2048, 2048], P(None, 'tp'), may hold values from -0.125 to 0.125
- key_weight: bfloat16 [2048, 256], replicated, may hold values from -0.125 to 0.125
- value_weight: bfloat16 [2048, 256], replicated, may hold values from -0.125 to 0.125
- output_weight: bfloat16 [2048, 2048], P('tp'), may hold values from -0.125 to 0.125
- saved_out: bfloat16 [1024, 2048], P(('grp', 'sp'), 'tp'), parts along dimension 0, may hold values from -3 to 3
- log_shift: float32 [16, 1024], P('tp', ('grp', 'sp')), parts along dimension 1, may hold values from 0 to 2
- out_grad: bfloat16 [1024, 2048], P(('grp', 'sp', 'tp')), parts along dimension 0, may hold values from -48 to 48
Outputs:
- target_grad: float32 [1024, 2048], P(('grp', 'sp', 'tp')), parts along dimension 0
- source_grad: float32 [8192, 2048], P(('grp', 'sp', 'tp')), parts along dimension 0
- query_weight_grad: float32 [4096, 2048], P(('grp', 'sp'), 'tp'), parts along dimension 0
There are 2 independent parts, one for each index of `grp`. A program takes and returns all parts, laid end to end along the dimension named above; an argument that names none is the same for every part. Nothing has to cross between parts.
All inputs are finite; a program needn't handle non-finite values.
Results may differ from a plain program's by a relative error of at most 0.02.
Values may be sent and summed in bfloat16 or wider, within the bound.
A program may use at most 64 MiB of HBM per device.

v0:
```python
import functools
import math

import jax
import jax.numpy as jnp
from jax import lax
from jax.experimental import pallas as pl
from jax.experimental.pallas import tpu as pltpu
from jax.sharding import PartitionSpec as P

HEADS = 16
HEAD_DIM = 128
KV_HEADS = 2
LOG2E = 1.4426950408889634
BF16 = jnp.bfloat16
F32 = jnp.float32


def rows_split(sp_count):
    keys = 2 if sp_count % 2 == 0 else 1
    while keys * keys * 4 <= sp_count:
        keys *= 2
    return keys, sp_count // keys


def dot_nt(a, b):
    return lax.dot_general(a, b, (((1,), (1,)), ((), ())), preferred_element_type=F32)


def dot_tn(a, b):
    return lax.dot_general(a, b, (((0,), (0,)), ((), ())), preferred_element_type=F32)


def flat_rows(block):
    count = block.shape[-2]
    shape = (-1, block.shape[-1])
    if count % 16:
        return block.astype(F32).reshape(shape).astype(BF16)
    return block.reshape(shape)


def kernel(
    sp_count,
    tp_count,
    log_rows,
    target,
    source,
    norm_gain,
    query_weight,
    key_weight,
    value_weight,
    output_weight,
    saved_out,
    log_shift,
    out_grad,
    target_grad,
    source_grad,
    query_weight_grad,
    tgt,
    src,
    gain,
    wq,
    wkv,
    wo,
    saved,
    shift,
    nbuf,
    obuf,
    kvown,
    kvbuf,
    qob,
    stat,
    nall,
    kacc,
    qacc,
    qfull,
    qsend,
    qrecv,
    qgall,
    ngf,
    ngs,
    ngr,
    ngx,
    ngin,
    kvs,
    kvr,
    kz,
    kzr,
    kfin,
    fin,
    ksum,
    in_sem,
    send_sem,
    recv_sem,
):
    nA, nB, nS, nT = kvbuf.shape[0], qob.shape[0], sp_count, tp_count
    nX = nT // 2
    nR = nT // KV_HEADS
    nr, width = tgt.shape
    sr = src.shape[0]
    lh = shift.shape[0]
    tr = saved.shape[0]
    trx = tr // nX
    ds_width = width // nS
    factor = HEAD_DIM ** (-0.5)
    s = lax.axis_index("sp")
    t = lax.axis_index("tp")
    x, c = t // 2, t % 2
    other = 1 - c
    part, pair = t % nR, t // nR
    zh, zl = s % nA, s // nA

    pending = []
    counts = {"send": 0, "recv": 0, "in": 0}

    def take(kind, n=1):
        first = counts[kind]
        counts[kind] += n
        return first

    def remote(src_ref, dst_ref, recv, where, keep=True):
        copy = pltpu.make_async_remote_copy(
            src_ref=src_ref,
            dst_ref=dst_ref,
            send_sem=send_sem.at[take("send")],
            recv_sem=recv_sem.at[recv],
            device_id=where,
            device_id_type=pl.DeviceIdType.MESH,
        )
        if keep:
            copy.start()
            pending.append(copy)
        return copy

    def arrive(dst_ref, recv, where):
        pltpu.make_async_remote_copy(
            src_ref=dst_ref,
            dst_ref=dst_ref,
            send_sem=send_sem.at[0],
            recv_sem=recv_sem.at[recv],
            device_id=where,
            device_id_type=pl.DeviceIdType.MESH,
        ).wait_recv()

    def fetch(src_ref, dst_ref):
        copy = pltpu.make_async_copy(src_ref, dst_ref, in_sem.at[take("in")])
        copy.start()
        return copy

    def tp_at(xx, cc):
        return {"tp": xx * 2 + cc}

    sibling = tp_at(x, other)

    got_t = fetch(target, tgt)
    got_g = fetch(norm_gain, gain)
    got_o = fetch(out_grad, obuf.at[x, c])
    got_kv = [fetch(source, src)]
    for g in range(KV_HEADS):
        cols = pl.ds(g * HEAD_DIM, HEAD_DIM)
        got_kv.append(fetch(key_weight.at[:, cols], wkv.at[:, pl.ds(2 * g * HEAD_DIM, HEAD_DIM)]))
        got_kv.append(
            fetch(value_weight.at[:, cols], wkv.at[:, pl.ds((2 * g + 1) * HEAD_DIM, HEAD_DIM)])
        )
    got_q = [
        fetch(query_weight, wq),
        fetch(output_weight, wo),
        fetch(saved_out, saved),
        fetch(log_shift, shift),
    ]

    barrier = pltpu.get_barrier_semaphore()
    for k in range(1, nT):
        pl.semaphore_signal(
            barrier, 1, device_id={"tp": (t + k) % nT}, device_id_type=pl.DeviceIdType.MESH
        )
    for k in range(1, nS):
        pl.semaphore_signal(
            barrier, 1, device_id={"sp": (s + k) % nS}, device_id_type=pl.DeviceIdType.MESH
        )

    got_t.wait()
    got_g.wait()
    wide = tgt[...].astype(F32)
    root = jnp.sqrt(jnp.mean(wide * wide, axis=1, keepdims=True) + 1e-06)
    nbuf[x, c] = (wide / root * gain[...]).astype(BF16)
    got_o.wait()
    pl.semaphore_wait(barrier, nT - 1 + nS - 1)

    n_recv = take("recv", 2 * nX)
    o_recv = take("recv", 2 * nX)
    bufs = ((nbuf, n_recv), (obuf, o_recv))
    for k in range(1, nX):
        for buf, base in bufs:
            remote(buf.at[x, c], buf.at[x, c], base + k, tp_at((x + k) % nX, c))
    for buf, base in bufs:
        remote(buf.at[x, c], buf.at[x, c], base, sibling)

    for copy in got_kv:
        copy.wait()
    own = jnp.dot(src[...], wkv[...], preferred_element_type=F32).astype(BF16)
    for g in range(KV_HEADS):
        kvown[g] = own[:, 2 * g * HEAD_DIM : 2 * (g + 1) * HEAD_DIM]
    kvbuf[0, t] = kvown[pair]
    kv_recv = take("recv", 2 * nX)
    for k in range(1, nX):
        xx = (x + k) % nX
        remote(kvown.at[xx * 2 // nR], kvbuf.at[0, t], kv_recv + k, tp_at(xx, c))
    remote(kvown.at[pair], kvbuf.at[0, t], kv_recv, sibling)
    kz_recv = take("recv", 2 * nA * nX)

    def keys_along(a_x, slot):
        for a in range(1, nA):
            remote(
                kvbuf.at[0, slot],
                kvbuf.at[a, slot],
                kz_recv + a * nX + a_x,
                {"sp": zl * nA + (zh + a) % nA},
            )

    keys_along(0, t)

    got_q[-1].wait()
    for xx in range(nX):
        for h in range(lh):
            cols = slice(h * trx, (h + 1) * trx)
            row = (shift[h : h + 1, xx * trx : (xx + 1) * trx] + log_rows) * LOG2E
            stat[0, xx, 0:1, cols] = row
    q_recv = take("recv", 2 * nB * nX)
    st_recv = take("recv", nB * nX)

    def project(k):
        xx = (x + nX - k) % nX
        q_rows = jnp.dot(flat_rows(nbuf[xx]), wq[...], preferred_element_type=F32).astype(BF16)
        for h in range(lh):
            cols = slice(h * HEAD_DIM, (h + 1) * HEAD_DIM)
            qob[0, xx, 0, h * trx : (h + 1) * trx, :] = q_rows[:, cols]
        for b in range(1, nB):
            where = {"sp": (zl + b) % nB * nA + zh}
            remote(qob.at[0, xx, 0], qob.at[b, xx, 0], q_recv + b * nX + k, where)
        o_rows = dot_nt(flat_rows(obuf[xx]), wo[...]).astype(BF16)
        keep = saved[pl.ds(pl.multiple_of(xx * trx, trx), trx), :].astype(F32)
        lane = lax.broadcasted_iota(jnp.int32, (trx, HEAD_DIM), 1)
        drops = jnp.zeros((trx, HEAD_DIM), F32)
        for h in range(lh):
            cols = slice(h * HEAD_DIM, (h + 1) * HEAD_DIM)
            rows = slice(h * trx, (h + 1) * trx)
            qob[0, xx, 1, rows, :] = o_rows[:, cols]
            term = jnp.sum(o_rows[:, cols].astype(F32) * keep[:, cols], axis=1, keepdims=True)
            drops = jnp.where(lane == h, term, drops)
        if trx < HEAD_DIM:
            drops = jnp.concatenate([drops, jnp.zeros((HEAD_DIM - trx, HEAD_DIM), F32)], axis=0)
        drops = drops.T
        for h in range(lh):
            stat[0, xx, 1:2, h * trx : (h + 1) * trx] = drops[h : h + 1, :trx]
        for b in range(1, nB):
            where = {"sp": (zl + b) % nB * nA + zh}
            remote(stat.at[0, xx], stat.at[b, xx], st_recv + b * nX + k, where)
            remote(qob.at[0, xx, 1], qob.at[b, xx, 1], q_recv + (nB + b) * nX + k, where)

    for copy in got_q[:-1]:
        copy.wait()
    for buf, base in bufs:
        arrive(buf.at[x, other], base, sibling)
    project(0)

    slots = [(b, a) for b in range(nB) for a in range(nA)]
    nz_recv = take("recv", nS * (1 + 2 * nX))

    def ahead(b, a):
        return (zl + b) % nB * nA + (zh + a) % nA

    def behind(b, a):
        return (zl + nB - b) % nB * nA + (zh + nA - a) % nA

    for n, (b, a) in enumerate(slots[1:], 1):
        to = ahead(b, a)
        cols = pl.ds(pl.multiple_of(to * ds_width, HEAD_DIM), ds_width)
        remote(nbuf.at[x, c, :, cols], nall.at[n, x, c], nz_recv + n, {"sp": to})

    for k in range(1, nX):
        xx = (x + nX - k) % nX
        for buf, base in bufs:
            arrive(buf.at[xx, c], base + k, tp_at(xx, c))
            remote(buf.at[xx, c], buf.at[xx, c], base + nX + k, sibling)
    for k in range(1, nX):
        xx = (x + nX - k) % nX
        for buf, base in bufs:
            arrive(buf.at[xx, other], base + nX + k, sibling)
        project(k)

    for k in range(1, nX):
        xx = (x + nX - k) % nX
        slot = xx * 2 + c
        arrive(kvbuf.at[0, slot], kv_recv + k, tp_at(xx, c))
        keys_along(k, slot)
        remote(kvbuf.at[0, slot], kvbuf.at[0, slot], kv_recv + nX + k, sibling)
    nall[0] = nbuf[:, :, :, pl.ds(pl.multiple_of(s * ds_width, HEAD_DIM), ds_width)]
    for k in range(1, nX):
        xx = (x + nX - k) % nX
        arrive(kvbuf.at[0, xx * 2 + other], kv_recv + nX + k, sibling)
    arrive(kvbuf.at[0, x * 2 + other], kv_recv, sibling)

    def attend(b, k, a):
        xx = (x + nX - k) % nX

        def step(i, carry):
            keys = kvbuf[a, i, :, :HEAD_DIM]
            values = kvbuf[a, i, :, HEAD_DIM:]
            queries = qob[b, xx, 0]
            backs = qob[b, xx, 1]
            score = dot_nt(keys, queries)
            prob = jnp.exp2(score * (factor * LOG2E) - stat[b, xx, 0:1, :])
            grad = (prob * (dot_nt(values, backs) - stat[b, xx, 1:2, :])).astype(BF16)
            key_part = jnp.dot(grad, queries, preferred_element_type=F32)
            value_part = jnp.dot(prob.astype(BF16), backs, preferred_element_type=F32)
            if b == 0 and k == 0:
                kacc[a, i, :, :HEAD_DIM] = key_part
                kacc[a, i, :, HEAD_DIM:] = value_part
            else:
                kacc[a, i, :, :HEAD_DIM] += key_part
                kacc[a, i, :, HEAD_DIM:] += value_part
            qacc[b, xx] += dot_tn(keys, grad)
            return carry

        lax.fori_loop(0, nT, step, 0, unroll=min(nT, 4))

    qs_recv = take("recv", nB * nB * nX)

    def send_queries(b, k):
        xx = (x + nX - k) % nX
        block = (qacc[b, xx] * factor).T
        qfull[b, xx] = block
        qsend[b, xx] = block.astype(BF16)
        for n in range(1, nB):
            slot = (n + b) % nB
            remote(
                qsend.at[b, xx],
                qrecv.at[n, slot, xx],
                qs_recv + (n * nB + slot) * nX + k,
                {"sp": (zl + n) % nB * nA + zh},
            )

    qacc[...] = jnp.zeros(qacc.shape, F32)
    for k in range(nX):
        attend(0, k, 0)

    for a in range(1, nA):
        for a_x in range(nX):
            slot = (x + nX - a_x) % nX * 2 + c
            idx = kz_recv + a * nX + a_x
            where = {"sp": zl * nA + (zh + nA - a) % nA}
            arrive(kvbuf.at[a, slot], idx, where)
            remote(kvbuf.at[a, slot], kvbuf.at[a, slot], idx + nA * nX, sibling)
        if a == 1:
            for n, (b, aa) in enumerate(slots[1:], 1):
                arrive(nall.at[n, x, c], nz_recv + n, {"sp": behind(b, aa)})
                base = nz_recv + nS + n * 2 * nX
                for j in range(1, nX):
                    remote(nall.at[n, x, c], nall.at[n, x, c], base + j, tp_at((x + j) % nX, c))
                remote(nall.at[n, x, c], nall.at[n, x, c], base, sibling)
        for a_x in range(nX):
            slot = (x + nX - a_x) % nX * 2 + other
            arrive(kvbuf.at[a, slot], kz_recv + a * nX + a_x + nA * nX, sibling)
        for k in range(nX):
            attend(0, k, a)
            if a == nA - 1:
                send_queries(0, k)

    kr_recv = take("recv", nA * nR)

    def send_keys(a):
        def convert(i, carry):
            kvs[a, i, :, :HEAD_DIM] = (kacc[a, i, :, :HEAD_DIM] * factor).astype(BF16)
            kvs[a, i, :, HEAD_DIM:] = kacc[a, i, :, HEAD_DIM:].astype(BF16)
            return carry

        lax.fori_loop(0, nT, convert, 0)
        for k in range(1, nR):
            to = (part + k) % nR
            remote(
                kvs.at[a, pl.ds(to * KV_HEADS, KV_HEADS)],
                kvr.at[k, a],
                kr_recv + a * nR + k,
                {"tp": pair * nR + to},
            )

    for k in range(nX):
        for b in range(1, nB):
            xx = (x + nX - k) % nX
            where = {"sp": (zl + nB - b) % nB * nA + zh}
            arrive(stat.at[b, xx], st_recv + b * nX + k, where)
            arrive(qob.at[b, xx, 0], q_recv + b * nX + k, where)
            arrive(qob.at[b, xx, 1], q_recv + (nB + b) * nX + k, where)
            last = k == nX - 1 and b == nB - 1
            for a in range(nA - 1, -1, -1):
                attend(b, k, a)
                if a == 0:
                    send_queries(b, k)
                if last:
                    send_keys(a)

    qg_recv = take("recv", nS)

    def finish_queries(b):
        for k in range(nX):
            xx = (x + nX - k) % nX
            total = qfull[b, xx]
            for n in range(1, nB):
                base = qs_recv + (n * nB + b) * nX + k
                arrive(qrecv.at[n, b, xx], base, {"sp": (zl + nB - n) % nB * nA + zh})
                total += qrecv[n, b, xx].astype(F32)
            total = total.astype(BF16)
            rows = pl.ds(pl.multiple_of(xx * trx, trx), trx)
            for h in range(lh):
                cols = slice(h * HEAD_DIM, (h + 1) * HEAD_DIM)
                qgall[b * nA, rows, cols] = total[h * trx : (h + 1) * trx, :]
        for a in range(1, nA):
            remote(
                qgall.at[b * nA],
                qgall.at[b * nA + a],
                qg_recv + b * nA + a,
                {"sp": zl * nA + (zh + a) % nA},
            )

    def portion(a, i):
        block = kacc[a, part * KV_HEADS + i]
        k_lane = lax.broadcasted_iota(jnp.int32, block.shape, 1) < HEAD_DIM
        block = jnp.where(k_lane, block * factor, block)
        for k in range(1, nR):
            block += kvr[k, a, i].astype(F32)
        return block

    ka_recv = take("recv", nA)
    for a in range(nA - 1, 0, -1):
        for k in range(1, nR):
            where = {"tp": pair * nR + (part + nR - k) % nR}
            arrive(kvr.at[k, a], kr_recv + a * nR + k, where)
        for i in range(KV_HEADS):
            kz[a, i] = portion(a, i).astype(BF16)
        remote(kz.at[a], kzr.at[a], ka_recv + a, {"sp": zl * nA + (zh + nA - a) % nA})

    for b in range(1, nB):
        finish_queries(b)

    for n, (b, a) in enumerate(slots[1:], 1):
        base = nz_recv + nS + n * 2 * nX
        for j in range(1, nX):
            xx = (x + nX - j) % nX
            arrive(nall.at[n, xx, c], base + j, tp_at(xx, c))
            remote(nall.at[n, xx, c], nall.at[n, xx, c], base + nX + j, sibling)

    finish_queries(0)

    step_cols = min(512, width)
    for i in range(width // step_cols):
        cols = slice(i * step_cols, (i + 1) * step_cols)
        share = dot_nt(qgall[0], wq[cols, :])
        ngf[:, :, :, cols] = share.reshape(nX, 2, nr, step_cols)
    for xx in range(nX):
        ngs[xx] = ngf[xx, other].astype(BF16)
    ng_recv = take("recv", nX)
    remote(ngs, ngr, ng_recv, sibling)

    for k in range(1, nR):
        arrive(kvr.at[k, 0], kr_recv + k, {"tp": pair * nR + (part + nR - k) % nR})
    for i in range(KV_HEADS):
        ksum[i] = portion(0, i)

    arrive(ngr, ng_recv, sibling)
    for k in range(1, nX):
        xx = (x + k) % nX
        ngx[k] = (ngf[xx, c] + ngr[xx].astype(F32)).astype(BF16)
        remote(ngx.at[k], ngin.at[k], ng_recv + k, tp_at(xx, c))

    for a in range(1, nA):
        arrive(kzr.at[a], ka_recv + a, {"sp": zl * nA + (zh + a) % nA})
    f_recv = take("recv", KV_HEADS)
    owner_sends = []
    for i in range(KV_HEADS):
        block = ksum[i]
        for a in range(1, nA):
            block += kzr[a, i].astype(F32)
        kfin[i] = block.astype(BF16)
        owner = part * KV_HEADS + i
        copy = remote(kfin.at[i], fin.at[pair], f_recv + pair, {"tp": owner}, keep=False)
        owner_sends.append((owner, copy))

        @pl.when(owner != t)
        def _():
            copy.start()

        @pl.when(owner == t)
        def _():
            fin[pair] = kfin[i]

    for n, (b, a) in enumerate(slots):
        if n:
            base = nz_recv + nS + n * 2 * nX
            arrive(nall.at[n, x, other], base, sibling)
            for j in range(1, nX):
                arrive(nall.at[n, (x + nX - j) % nX, other], base + nX + j, sibling)
    order = [b * nA for b in range(nB)] + [b * nA + a for b in list(range(1, nB)) + [0] for a in range(1, nA)]
    for n in order:
        if n % nA:
            arrive(qgall.at[n], qg_recv + n, {"sp": zl * nA + (zh + nA - n % nA) % nA})
        piece = dot_tn(flat_rows(nall[n]), qgall[n])
        if n == 0:
            query_weight_grad[...] = piece
        else:
            query_weight_grad[...] += piece

    grad = ngf[x, c] + ngr[x].astype(F32)
    for k in range(1, nX):
        arrive(ngin.at[k], ng_recv + k, tp_at((x + nX - k) % nX, c))
        grad += ngin[k].astype(F32)
    scaled = grad * gain[...]
    wide = tgt[...].astype(F32)
    root = jnp.sqrt(jnp.mean(wide * wide, axis=1, keepdims=True) + 1e-06)
    target_grad[...] = scaled / root - wide * jnp.mean(scaled * wide, axis=1, keepdims=True) / (
        root * root * root
    )

    for g in range(KV_HEADS):
        giver = g * nR + t // KV_HEADS

        @pl.when(giver != t)
        def _():
            arrive(fin.at[g], f_recv + g, {"tp": giver})

    for i in range(width // step_cols):
        rows = pl.ds(i * step_cols, step_cols)
        part_sum = dot_nt(fin[0], wkv[rows, 0 : 2 * HEAD_DIM])
        for g in range(1, KV_HEADS):
            part_sum += dot_nt(fin[g], wkv[rows, 2 * g * HEAD_DIM : 2 * (g + 1) * HEAD_DIM])
        source_grad[:, rows] = part_sum

    for copy in pending:
        copy.wait_send()
    for owner, copy in owner_sends:

        @pl.when(owner != t)
        def _():
            copy.wait_send()


def shards(
    target,
    source,
    norm_gain,
    query_weight,
    key_weight,
    value_weight,
    output_weight,
    saved_out,
    log_shift,
    out_grad,
):
    nT = lax.axis_size("tp")
    nS = lax.axis_size("sp")
    nA, nB = rows_split(nS)
    nX, nR = nT // 2, nT // KV_HEADS
    nr, width = target.shape
    sr = source.shape[0]
    tr, head_width = saved_out.shape
    lh = head_width // HEAD_DIM
    m = lh * tr // nX
    ds_width = width // nS
    kv = 2 * HEAD_DIM
    log_rows = math.log(sr * nT * nS)
    vm = pltpu.VMEM
    outputs = 4 * (nr * width + sr * width + ds_width * head_width)
    limit = 67043328 - outputs - 65536
    sems = min(8 * nS * nT, 1024)
    scratch = [
        vm((nr, width), BF16),
        vm((sr, width), BF16),
        vm((1, width), F32),
        vm((width, head_width), BF16),
        vm((width, KV_HEADS * kv), BF16),
        vm((head_width, width), BF16),
        vm((tr, head_width), BF16),
        vm((lh, tr), F32),
        vm((nX, 2, nr, width), BF16),
        vm((nX, 2, nr, width), BF16),
        vm((KV_HEADS, sr, kv), BF16),
        vm((nA, nT, sr, kv), BF16),
        vm((nB, nX, 2, m, HEAD_DIM), BF16),
        vm((nB, nX, 2, m), F32),
        vm((nS, nX, 2, nr, ds_width), BF16),
        vm((nA, nT, sr, kv), F32),
        vm((nB, nX, HEAD_DIM, m), F32),
        vm((nB, nX, m, HEAD_DIM), F32),
        vm((nB, nX, m, HEAD_DIM), BF16),
        vm((nB, nB, nX, m, HEAD_DIM), BF16),
        vm((nS, tr, head_width), BF16),
        vm((nX, 2, nr, width), F32),
        vm((nX, nr, width), BF16),
        vm((nX, nr, width), BF16),
        vm((nX, nr, width), BF16),
        vm((nX, nr, width), BF16),
        vm((nA, nT, sr, kv), BF16),
        vm((nR, nA, KV_HEADS, sr, kv), BF16),
        vm((nA, KV_HEADS, sr, kv), BF16),
        vm((nA, KV_HEADS, sr, kv), BF16),
        vm((KV_HEADS, sr, kv), BF16),
        vm((KV_HEADS, sr, kv), BF16),
        vm((KV_HEADS, sr, kv), F32),
        pltpu.SemaphoreType.DMA((16,)),
        pltpu.SemaphoreType.DMA((sems,)),
        pltpu.SemaphoreType.DMA((sems,)),
    ]
    anywhere = pl.BlockSpec(memory_space=pltpu.HBM)
    return pl.pallas_call(
        functools.partial(kernel, nS, nT, log_rows),
        out_shape=(
            pltpu.VMEM((nr, width), F32),
            pltpu.VMEM((sr, width), F32),
            pltpu.VMEM((ds_width, head_width), F32),
        ),
        in_specs=[anywhere] * 10,
        out_specs=(pl.BlockSpec(memory_space=pltpu.VMEM),) * 3,
        scratch_shapes=scratch,
        compiler_params=pltpu.CompilerParams(
            collective_id=0, has_side_effects=True, vmem_limit_bytes=limit
        ),
        name="cross_back",
    )(
        target,
        source,
        norm_gain.reshape(1, width),
        query_weight,
        key_weight,
        value_weight,
        output_weight,
        saved_out,
        log_shift,
        out_grad,
    )


def solution(mesh):
    return jax.shard_map(
        shards,
        mesh=mesh,
        in_specs=(
            P(("grp", "sp", "tp"), None),
            P(("grp", "sp", "tp"), None),
            P(),
            P(None, "tp"),
            P(),
            P(),
            P("tp", None),
            P(("grp", "sp"), "tp"),
            P("tp", ("grp", "sp")),
            P(("grp", "sp", "tp"), None),
        ),
        out_specs=(
            P(("grp", "sp", "tp"), None),
            P(("grp", "sp", "tp"), None),
            P(("grp", "sp"), "tp"),
        ),
        check_vma=False,
    )
```

profile of v0, /device:TPU:1, one launch (start us, length us, event | category | flops | bytes accessed | tf_op | source)
XLA Modules:
  0.0 54.1 jit_solution(17511749245309820295)
XLA Ops:
  0.6 50.5 %cross_back.1 = (f32[32,2048]{1,0:T(8,128)S(1)}, f32[256,2048]{1,0:T(8,128)S(1)}, f32[512,512]{1,0:T(8,128)S(1)}) custom-call(bf16[32,2048]{1,0:T(8,128)(2,1)} %target.1, bf16[256,2048]{1,0:T(8,128)(2,1)} %source.1, f32[1,2048]{1,0:T(1,128)} %bitcast.1, bf16[2048,512]{1,0:T(8,128)(2,1)} %query_weight.1, bf16[2048,256]{1,0:T(8,128)(2,1)} %key_weight.1, ...), custom_call_target="tpu_custom_call" | custom-call | tf_op jit(solution)/shard_map/cross_back/pallas_call | solution.py:614
  51.1 0.7 %copy.16 = f32[32,2048]{1,0:T(8,128)} copy(f32[32,2048]{1,0:T(8,128)S(1)} %get-tuple-element.3) | data formatting | bytes 524288
  51.9 1.0 %copy.18 = f32[512,512]{1,0:T(8,128)} copy(f32[512,512]{1,0:T(8,128)S(1)} %get-tuple-element.5) | data formatting | bytes 2097152
  52.8 1.3 %copy.17 = f32[256,2048]{1,0:T(8,128)} copy(f32[256,2048]{1,0:T(8,128)S(1)} %get-tuple-element.4) | data formatting | bytes 4194304
where the time goes:
time: 54.9 us; the launch traced here: 54.1 us
  Pallas kernels  50.5 us (92%)
  local copies, waits for them, and re-layouts  2.99 us (5%)
  between operations  0.64 us (1%)
    pallas_call x1, Pallas kernels, shards(): pl.pallas_call(functools.partial(kernel, nS, nT, log_rows), out_shape=(pl...  50.5 us
    unnamed x3, local copies, waits for them, and re-layouts  2.99 us

commit v1 on v0

--- a/solution.py
+++ b/solution.py
@@ -544,6 +544,560 @@
             copy.wait_send()
 
 
+def square_kernel(
+    log_rows,
+    target,
+    source,
+    norm_gain,
+    query_weight,
+    key_weight,
+    value_weight,
+    output_weight,
+    saved_out,
+    log_shift,
+    out_grad,
+    target_grad,
+    source_grad,
+    query_weight_grad,
+    tgt,
+    src,
+    gain,
+    wq,
+    wkv,
+    wo,
+    saved,
+    shift,
+    nbuf,
+    obuf,
+    kvown,
+    kvbuf,
+    kvpeer,
+    qob,
+    stat,
+    nall,
+    kacc,
+    qacc,
+    qfull,
+    qsend,
+    qrecv,
+    qgall,
+    ngf,
+    ngs,
+    ngr,
+    ngx,
+    ngin,
+    kvs,
+    kvr,
+    kz,
+    kzr,
+    kfin,
+    fin,
+    in_sem,
+    send_sem,
+    recv_sem,
+):
+    nr, width = tgt.shape
+    lh = shift.shape[0]
+    tr = saved.shape[0]
+    nS, nT = 4, 4
+    trx = tr // 2
+    ds_width = width // nS
+    factor = HEAD_DIM ** (-0.5)
+    s = lax.axis_index("sp")
+    t = lax.axis_index("tp")
+    x, c = t // 2, t % 2
+    ox, other = 1 - x, 1 - c
+    peer = s + 1 - 2 * (s % 2)
+    far = (s + 2) % nS
+    diag = (peer + 2) % nS
+    sib = {"tp": x * 2 + other}
+    across = {"tp": ox * 2 + c}
+    to_peer = {"sp": peer}
+    to_far = {"sp": far}
+    to_diag = {"sp": diag}
+
+    keys = {("fin", 0): 0, ("fin", 1): 1}
+    counts = {"in": 0}
+
+    def sem(*key):
+        return keys.setdefault(key, len(keys))
+
+    def fetch(src_ref, dst_ref):
+        copy = pltpu.make_async_copy(src_ref, dst_ref, in_sem.at[counts["in"]])
+        counts["in"] += 1
+        copy.start()
+        return copy
+
+    got_t = fetch(target, tgt)
+    got_g = fetch(norm_gain, gain)
+    got_shift = fetch(log_shift, shift)
+    got_o = fetch(out_grad, obuf.at[x, c])
+    got_kv = [fetch(source, src)]
+    for g in range(KV_HEADS):
+        cols = pl.ds(g * HEAD_DIM, HEAD_DIM)
+        got_kv.append(fetch(key_weight.at[:, cols], wkv.at[:, pl.ds(2 * g * HEAD_DIM, HEAD_DIM)]))
+        got_kv.append(
+            fetch(value_weight.at[:, cols], wkv.at[:, pl.ds((2 * g + 1) * HEAD_DIM, HEAD_DIM)])
+        )
+    got_q = fetch(query_weight, wq)
+    got_w = fetch(output_weight, wo)
+    got_saved = fetch(saved_out, saved)
+
+    barrier = pltpu.get_barrier_semaphore()
+    for k in range(1, nT):
+        pl.semaphore_signal(
+            barrier, 1, device_id={"tp": (t + k) % nT}, device_id_type=pl.DeviceIdType.MESH
+        )
+    for k in range(1, nS):
+        pl.semaphore_signal(
+            barrier, 1, device_id={"sp": (s + k) % nS}, device_id_type=pl.DeviceIdType.MESH
+        )
+
+    got_t.wait()
+    got_g.wait()
+    wide = tgt[...].astype(F32)
+    root = jnp.sqrt(jnp.mean(wide * wide, axis=1, keepdims=True) + 1e-06)
+    nbuf[x, c] = (wide / root * gain[...]).astype(BF16)
+    got_o.wait()
+    pl.semaphore_wait(barrier, nT - 1 + nS - 1)
+
+    pending = []
+
+    def remote(src_ref, dst_ref, key, where, keep=True):
+        copy = pltpu.make_async_remote_copy(
+            src_ref=src_ref,
+            dst_ref=dst_ref,
+            send_sem=send_sem.at[len(pending)],
+            recv_sem=recv_sem.at[sem(*key) if isinstance(key, tuple) else key],
+            device_id=where,
+            device_id_type=pl.DeviceIdType.MESH,
+        )
+        if keep:
+            copy.start()
+        pending.append((copy, keep))
+        return copy
+
+    def arrive(dst_ref, key, where):
+        pltpu.make_async_remote_copy(
+            src_ref=dst_ref,
+            dst_ref=dst_ref,
+            send_sem=send_sem.at[0],
+            recv_sem=recv_sem.at[sem(*key)],
+            device_id=where,
+            device_id_type=pl.DeviceIdType.MESH,
+        ).wait_recv()
+
+    def scope(name):
+        return jax.named_scope(name)
+
+    remote(nbuf.at[x, c], nbuf.at[x, c], ("n", "x"), across)
+    remote(nbuf.at[x, c], nbuf.at[x, c], ("n", "s"), sib)
+    remote(obuf.at[x, c], obuf.at[x, c], ("o", "s"), sib)
+    remote(obuf.at[x, c], obuf.at[x, c], ("o", "x"), across)
+    for copy in got_kv:
+        copy.wait()
+    with scope("kvproj"):
+        own = jnp.dot(src[...], wkv[...], preferred_element_type=F32).astype(BF16)
+        for g in range(KV_HEADS):
+            kvown[g] = own[:, 2 * g * HEAD_DIM : 2 * (g + 1) * HEAD_DIM]
+        kvbuf[0, t] = kvown[x]
+    remote(kvown.at[x], kvbuf.at[0, t], ("kv", "s"), sib)
+    remote(kvown.at[ox], kvbuf.at[0, t], ("kv", "x"), across)
+    got_shift.wait()
+    for k in range(2):
+        xx = x if k == 0 else ox
+        for h in range(lh):
+            row = jnp.where(xx == 0, shift[h : h + 1, 0:trx], shift[h : h + 1, trx : 2 * trx])
+            stat[0, k, 0:1, h * trx : (h + 1) * trx] = (row + log_rows) * LOG2E
+
+    def send_far(ref, kind, k):
+        remote(ref.at[0, k], ref.at[1, k], (kind, k), to_far)
+
+    def send_part(i, kind, k):
+        remote(qob.at[0, k, i], qob.at[1, k, i], (kind, k), to_far)
+
+    def project_q(k):
+        with scope(f"project_q{k}"):
+            xx = x if k == 0 else ox
+            rows = jnp.dot(flat_rows(nbuf[xx]), wq[...], preferred_element_type=F32).astype(BF16)
+            for h in range(lh):
+                cols = slice(h * HEAD_DIM, (h + 1) * HEAD_DIM)
+                qob[0, k, 0, h * trx : (h + 1) * trx, :] = rows[:, cols]
+        send_part(0, "q", k)
+
+    def project_o(k):
+        with scope(f"project_o{k}"):
+            xx = x if k == 0 else ox
+            o_rows = dot_nt(flat_rows(obuf[xx]), wo[...]).astype(BF16)
+            for h in range(lh):
+                cols = slice(h * HEAD_DIM, (h + 1) * HEAD_DIM)
+                qob[0, k, 1, h * trx : (h + 1) * trx, :] = o_rows[:, cols]
+        send_part(1, "ob", k)
+        with scope(f"drop{k}"):
+            keep = saved[pl.ds(pl.multiple_of(xx * trx, trx), trx), :].astype(F32)
+            lane = lax.broadcasted_iota(jnp.int32, (trx, HEAD_DIM), 1)
+            drops = jnp.zeros((trx, HEAD_DIM), F32)
+            for h in range(lh):
+                cols = slice(h * HEAD_DIM, (h + 1) * HEAD_DIM)
+                term = jnp.sum(o_rows[:, cols].astype(F32) * keep[:, cols], axis=1, keepdims=True)
+                drops = jnp.where(lane == h, term, drops)
+            drops = jnp.concatenate([drops, jnp.zeros((HEAD_DIM - trx, HEAD_DIM), F32)], axis=0)
+            drops = drops.T
+            for h in range(lh):
+                stat[0, k, 1:2, h * trx : (h + 1) * trx] = drops[h : h + 1, :trx]
+        send_far(stat, "st", k)
+
+    def need(k):
+        with scope(f"w_q{k}"):
+            arrive(qob.at[1, k, 0], ("q", k), to_far)
+        with scope(f"w_ob{k}"):
+            arrive(qob.at[1, k, 1], ("ob", k), to_far)
+            arrive(stat.at[1, k], ("st", k), to_far)
+
+    got = {"kacc": set(), "qacc": set()}
+
+    def attend(v, k, a, g):
+        with scope(f"attend_{v}{k}{a}{g}"):
+            attend_rows(v, k, a, g)
+
+    def attend_rows(v, k, a, g):
+        pair = pl.ds(2 * (x if g == 0 else ox), 2)
+        sr = kvbuf.shape[2]
+        k_rows = kvbuf[a, pair, :, :HEAD_DIM].reshape(2 * sr, HEAD_DIM)
+        v_rows = kvbuf[a, pair, :, HEAD_DIM:].reshape(2 * sr, HEAD_DIM)
+        queries = qob[v, k, 0]
+        backs = qob[v, k, 1]
+        score = dot_nt(k_rows, queries)
+        prob = jnp.exp2(score * (factor * LOG2E) - stat[v, k, 0:1, :])
+        grad = (prob * (dot_nt(v_rows, backs) - stat[v, k, 1:2, :])).astype(BF16)
+        key_part = jnp.dot(grad, queries, preferred_element_type=F32)
+        value_part = jnp.dot(prob.astype(BF16), backs, preferred_element_type=F32)
+        key_part = key_part.reshape(2, sr, HEAD_DIM)
+        value_part = value_part.reshape(2, sr, HEAD_DIM)
+        if (a, g) not in got["kacc"]:
+            kacc[a, pair, :, :HEAD_DIM] = key_part
+            kacc[a, pair, :, HEAD_DIM:] = value_part
+        else:
+            kacc[a, pair, :, :HEAD_DIM] += key_part
+            kacc[a, pair, :, HEAD_DIM:] += value_part
+        if (v, k) not in got["qacc"]:
+            qacc[v, k] = dot_tn(k_rows, grad)
+            got["qacc"].add((v, k))
+        else:
+            qacc[v, k] += dot_tn(k_rows, grad)
+        got["kacc"].add((a, g))
+
+    def query_part(v, k):
+        return (qacc[v, k] * factor).T
+
+    def send_keys(a):
+        with scope(f"keys{a}"):
+            for i in range(2):
+                slot = 2 * other + i
+                kvs[a, i, :, :HEAD_DIM] = (kacc[a, slot, :, :HEAD_DIM] * factor).astype(BF16)
+                kvs[a, i, :, HEAD_DIM:] = kacc[a, slot, :, HEAD_DIM:].astype(BF16)
+        remote(kvs.at[a], kvr.at[a], ("kp", a), sib)
+
+    def key_sum(a, i):
+        block = kacc[a, 2 * c + i]
+        k_lane = lax.broadcasted_iota(jnp.int32, block.shape, 1) < HEAD_DIM
+        return jnp.where(k_lane, block * factor, block) + kvr[a, i].astype(F32)
+
+    def keys_back():
+        with scope("w_kp1"):
+            arrive(kvr.at[1], ("kp", 1), sib)
+        with scope("kz"):
+            for i in range(2):
+                kz[i] = key_sum(1, i).astype(BF16)
+        remote(kz, kzr, ("kz",), to_peer)
+
+    def slice_sends():
+        for v, where, to in ((2, to_peer, peer), (1, to_far, far), (3, to_diag, diag)):
+            cols = pl.ds(pl.multiple_of(to * ds_width, HEAD_DIM), ds_width)
+            remote(nbuf.at[x, c, :, cols], nall.at[v, x, c], ("na", v), where)
+
+    def slice_from(v):
+        return (None, to_far, to_peer, to_diag)[v]
+
+    def slice_pass(v):
+        with scope(f"w_na{v}"):
+            arrive(nall.at[v, x, c], ("na", v), slice_from(v))
+        remote(nall.at[v, x, c], nall.at[v, x, c], ("na", v, "x"), across)
+        remote(nall.at[v, x, c], nall.at[v, x, c], ("na", v, "s"), sib)
+
+    def slice_turn(v):
+        with scope(f"w_nx{v}"):
+            arrive(nall.at[v, ox, c], ("na", v, "x"), across)
+        remote(nall.at[v, ox, c], nall.at[v, ox, c], ("na", v, "t"), sib)
+
+    def slice_end(v):
+        with scope(f"w_ns{v}"):
+            arrive(nall.at[v, x, other], ("na", v, "s"), sib)
+            arrive(nall.at[v, ox, other], ("na", v, "t"), sib)
+
+    def total_rows(v, k):
+        xx = x if k == 0 else ox
+        return qgall.at[v, pl.ds(pl.multiple_of(xx * trx, trx), trx), :]
+
+    pieces = []
+
+    def weight_piece(v):
+        with scope(f"piece{v}"):
+            piece = dot_tn(flat_rows(nall[v]), qgall[v])
+            if not pieces:
+                query_weight_grad[...] = piece
+            else:
+                query_weight_grad[...] += piece
+            pieces.append(v)
+
+    step_cols = min(512, width)
+
+    def normed_share():
+        with scope("ng_share"):
+            for i in range(width // step_cols):
+                cols = slice(i * step_cols, (i + 1) * step_cols)
+                share = dot_nt(qgall[0], wq[cols, :])
+                ngf[:, :, :, cols] = share.reshape(2, 2, nr, step_cols)
+            for xx in range(2):
+                ngs[xx] = ngf[xx, other].astype(BF16)
+        remote(ngs, ngr, ("ng", "s"), sib)
+
+    def normed_cross():
+        with scope("w_ngs"):
+            arrive(ngr, ("ng", "s"), sib)
+        ngx[...] = (ngf[ox, c] + ngr[ox].astype(F32)).astype(BF16)
+        remote(ngx, ngin, ("ng", "x"), across)
+
+    def normed_end():
+        with scope("w_ngx"):
+            arrive(ngin, ("ng", "x"), across)
+        with scope("target"):
+            grad = ngf[x, c] + ngr[x].astype(F32) + ngin[...].astype(F32)
+            scaled = grad * gain[...]
+            wide = tgt[...].astype(F32)
+            root = jnp.sqrt(jnp.mean(wide * wide, axis=1, keepdims=True) + 1e-06)
+            target_grad[...] = scaled / root - wide * jnp.mean(
+                scaled * wide, axis=1, keepdims=True
+            ) / (root * root * root)
+
+    owner_sends = []
+
+    def keys_out():
+        with scope("w_kp0"):
+            arrive(kvr.at[0], ("kp", 0), sib)
+        with scope("w_kz"):
+            arrive(kzr, ("kz",), to_peer)
+        with scope("keys_out"):
+            for i in range(2):
+                block = key_sum(0, i) + kzr[i].astype(F32)
+                kfin[i] = block.astype(BF16)
+                owner = c * 2 + i
+                copy = remote(kfin.at[i], fin.at[x], x, {"tp": owner}, keep=False)
+                owner_sends.append((owner, copy))
+
+                @pl.when(owner != t)
+                def _():
+                    copy.start()
+
+                @pl.when(owner == t)
+                def _():
+                    fin[x] = kfin[i]
+
+    def source_end():
+        for g in range(KV_HEADS):
+            giver = g * 2 + t // 2
+
+            @pl.when(giver != t)
+            def _():
+                with scope("w_fin"):
+                    arrive(fin.at[g], ("fin", g), {"tp": giver})
+
+        with scope("source"):
+            for i in range(width // step_cols):
+                rows = pl.ds(i * step_cols, step_cols)
+                part_sum = dot_nt(fin[0], wkv[rows, 0 : 2 * HEAD_DIM])
+                for g in range(1, KV_HEADS):
+                    part_sum += dot_nt(fin[g], wkv[rows, 2 * g * HEAD_DIM : 2 * (g + 1) * HEAD_DIM])
+                source_grad[:, rows] = part_sum
+
+    def pass_on(buf, kind):
+        with scope(f"w_{kind}x"):
+            arrive(buf.at[ox, c], (kind, "x"), across)
+        remote(buf.at[ox, c], buf.at[ox, c], (kind, "t"), sib)
+
+    def passed(buf, kind):
+        with scope(f"w_{kind}t"):
+            arrive(buf.at[ox, other], (kind, "t"), sib)
+
+    def grad_out(b, k):
+        with scope(f"dq_{b}{k}"):
+            block = query_part(b, k)
+            qfull[b, k] = block
+            qsend[b, k] = block.astype(BF16)
+        remote(qsend.at[b, k], qrecv.at[1 - b, k], ("dq", 1 - b, k), to_far)
+
+    def total_out(b, k):
+        with scope(f"w_dq{b}{k}"):
+            arrive(qrecv.at[b, k], ("dq", b, k), to_far)
+        with scope(f"total_{b}{k}"):
+            total = (qfull[b, k] + qrecv[b, k].astype(F32)).astype(BF16)
+            rows = pl.ds(pl.multiple_of((x if k == 0 else ox) * trx, trx), trx)
+            for h in range(lh):
+                cols = slice(h * HEAD_DIM, (h + 1) * HEAD_DIM)
+                qgall[b, rows, cols] = total[h * trx : (h + 1) * trx, :]
+        remote(total_rows(b, k), total_rows(2 + b, k), ("tot", b, k), to_peer)
+
+    def total_in(b, k):
+        with scope(f"w_tot{b}{k}"):
+            arrive(total_rows(2 + b, k), ("tot", b, k), to_peer)
+
+    def peer_keys(chip, kind):
+        with scope(f"w_{kind}"):
+            arrive(kvbuf.at[1, 2 * chip + c], (kind,), to_peer if chip is x else across)
+        remote(kvbuf.at[1, 2 * chip + c], kvbuf.at[1, 2 * chip + c], (kind, "s"), sib)
+
+    def peer_keys_end(chip, kind):
+        with scope(f"w_{kind}s"):
+            arrive(kvbuf.at[1, 2 * chip + other], (kind, "s"), sib)
+
+    remote(kvown.at[x], kvbuf.at[1, t], ("ke",), to_peer)
+    remote(kvown.at[ox], kvpeer, ("kp",), to_peer)
+    with scope("w_ns"):
+        arrive(nbuf.at[x, other], ("n", "s"), sib)
+    got_q.wait()
+    project_q(0)
+    with scope("w_os"):
+        arrive(obuf.at[x, other], ("o", "s"), sib)
+    got_w.wait()
+    got_saved.wait()
+    project_o(0)
+    with scope("w_kvs"):
+        arrive(kvbuf.at[0, x * 2 + other], ("kv", "s"), sib)
+    attend(0, 0, 0, 0)
+    pass_on(nbuf, "n")
+    peer_keys(x, "ke")
+    passed(nbuf, "n")
+    project_q(1)
+    peer_keys_end(x, "ke")
+    attend(0, 0, 1, 0)
+    pass_on(obuf, "o")
+    with scope("w_kpx"):
+        arrive(kvpeer, ("kp",), to_peer)
+    remote(kvpeer, kvbuf.at[1, t], ("kx",), across)
+    passed(obuf, "o")
+    project_o(1)
+    slice_sends()
+    attend(0, 1, 0, 0)
+    attend(0, 1, 1, 0)
+    with scope("w_kvx"):
+        arrive(kvbuf.at[0, 2 * ox + c], ("kv", "x"), across)
+    remote(kvbuf.at[0, 2 * ox + c], kvbuf.at[0, 2 * ox + c], ("kv", "t"), sib)
+    need(0)
+    attend(1, 0, 0, 0)
+    attend(1, 0, 1, 0)
+    with scope("w_kvt"):
+        arrive(kvbuf.at[0, 2 * ox + other], ("kv", "t"), sib)
+    attend(1, 0, 0, 1)
+    attend(0, 0, 0, 1)
+    peer_keys(ox, "kx")
+    attend(0, 1, 0, 1)
+    peer_keys_end(ox, "kx")
+    attend(1, 0, 1, 1)
+    grad_out(1, 0)
+    attend(0, 0, 1, 1)
+    grad_out(0, 0)
+    attend(0, 1, 1, 1)
+    need(1)
+    attend(1, 1, 1, 0)
+    attend(1, 1, 1, 1)
+    send_keys(1)
+    attend(1, 1, 0, 0)
+    attend(1, 1, 0, 1)
+    grad_out(1, 1)
+    send_keys(0)
+    keys_back()
+    grad_out(0, 1)
+    for v in (1, 2, 3):
+        slice_pass(v)
+    nall[0] = nbuf[:, :, :, pl.ds(pl.multiple_of(s * ds_width, HEAD_DIM), ds_width)]
+    total_out(0, 0)
+    total_out(1, 0)
+    for v in (1, 2, 3):
+        slice_turn(v)
+    total_out(0, 1)
+    normed_share()
+    for v in (1, 2, 3):
+        slice_end(v)
+    weight_piece(0)
+    normed_cross()
+    total_out(1, 1)
+    weight_piece(1)
+    keys_out()
+    total_in(0, 0)
+    total_in(1, 0)
+    total_in(0, 1)
+    weight_piece(2)
+    normed_end()
+    source_end()
+    total_in(1, 1)
+    weight_piece(3)
+
+    with scope("w_send"):
+        for copy, kept in pending:
+            if kept:
+                copy.wait_send()
+        for owner, copy in owner_sends:
+
+            @pl.when(owner != t)
+            def _():
+                copy.wait_send()
+
+
+def square_scratch(nr, width, sr, tr, lh, head_width):
+    vm = pltpu.VMEM
+    m = lh * tr // 2
+    ds_width = width // 4
+    kv = 2 * HEAD_DIM
+    return [
+        vm((nr, width), BF16),
+        vm((sr, width), BF16),
+        vm((1, width), F32),
+        vm((width, head_width), BF16),
+        vm((width, KV_HEADS * kv), BF16),
+        vm((head_width, width), BF16),
+        vm((tr, head_width), BF16),
+        vm((lh, tr), F32),
+        vm((2, 2, nr, width), BF16),
+        vm((2, 2, nr, width), BF16),
+        vm((KV_HEADS, sr, kv), BF16),
+        vm((2, 4, sr, kv), BF16),
+        vm((sr, kv), BF16),
+        vm((2, 2, 2, m, HEAD_DIM), BF16),
+        vm((2, 2, 2, m), F32),
+        vm((4, 2, 2, nr, ds_width), BF16),
+        vm((2, 4, sr, kv), F32),
+        vm((2, 2, HEAD_DIM, m), F32),
+        vm((2, 2, m, HEAD_DIM), F32),
+        vm((2, 2, m, HEAD_DIM), BF16),
+        vm((2, 2, m, HEAD_DIM), BF16),
+        vm((4, tr, head_width), BF16),
+        vm((2, 2, nr, width), F32),
+        vm((2, nr, width), BF16),
+        vm((2, nr, width), BF16),
+        vm((nr, width), BF16),
+        vm((nr, width), BF16),
+        vm((2, 2, sr, kv), BF16),
+        vm((2, 2, sr, kv), BF16),
+        vm((2, sr, kv), BF16),
+        vm((2, sr, kv), BF16),
+        vm((2, sr, kv), BF16),
+        vm((2, sr, kv), BF16),
+        pltpu.SemaphoreType.DMA((12,)),
+        pltpu.SemaphoreType.DMA((74,)),
+        pltpu.SemaphoreType.DMA((80,)),
+    ]
+
+
 def shards(
     target,
     source,
@@ -610,9 +1164,13 @@
         pltpu.SemaphoreType.DMA((sems,)),
         pltpu.SemaphoreType.DMA((sems,)),
     ]
+    body = functools.partial(kernel, nS, nT, log_rows)
+    if nS == 4 and nT == 4:
+        body = functools.partial(square_kernel, log_rows)
+        scratch = square_scratch(nr, width, sr, tr, lh, head_width)
     anywhere = pl.BlockSpec(memory_space=pltpu.HBM)
     return pl.pallas_call(
-        functools.partial(kernel, nS, nT, log_rows),
+        body,
         out_shape=(
             pltpu.VMEM((nr, width), F32),
             pltpu.VMEM((sr, width), F32),

time: 54.9 us -> 49.3 us (0.90); the launches traced: 54.1 us -> 49.1 us
  Pallas kernels: 50.5 us -> 45.5 us
    pallas_call x1, Pallas kernels: 50.5 us -> 45.5 us  [shards(): pl.pallas_call(body, out_shape=(pltpu.VMEM((nr, width), F32), pltpu.VMEM(...]
where the time goes in v1:
time: 49.3 us; the launch traced here: 49.1 us
  Pallas kernels  45.5 us (92%)
  local copies, waits for them, and re-layouts  2.99 us (6%)
  between operations  0.64 us (1%)
    pallas_call x1, Pallas kernels, shards(): pl.pallas_call(body, out_shape=(pltpu.VMEM((nr, width), F32), pltpu.VMEM(...  45.5 us
    unnamed x3, local copies, waits for them, and re-layouts  2.99 us

profile of v1, /device:TPU:1, one launch (start us, length us, event | category | flops | bytes accessed | tf_op | source)
XLA Modules:
  0.0 49.1 jit_solution(18217227872301901647)
XLA Ops:
  0.6 45.5 %cross_back.1 = (f32[32,2048]{1,0:T(8,128)S(1)}, f32[256,2048]{1,0:T(8,128)S(1)}, f32[512,512]{1,0:T(8,128)S(1)}) custom-call(bf16[32,2048]{1,0:T(8,128)(2,1)} %target.1, bf16[256,2048]{1,0:T(8,128)(2,1)} %source.1, f32[1,2048]{1,0:T(1,128)} %bitcast.1, bf16[2048,512]{1,0:T(8,128)(2,1)} %query_weight.1, bf16[2048,256]{1,0:T(8,128)(2,1)} %key_weight.1, ...), custom_call_target="tpu_custom_call" | custom-call | tf_op jit(solution)/shard_map/cross_back/pallas_call | solution.py:1172
  46.1 0.7 %copy.16 = f32[32,2048]{1,0:T(8,128)} copy(f32[32,2048]{1,0:T(8,128)S(1)} %get-tuple-element.3) | data formatting | bytes 524288
  46.8 1.0 %copy.18 = f32[512,512]{1,0:T(8,128)} copy(f32[512,512]{1,0:T(8,128)S(1)} %get-tuple-element.5) | data formatting | bytes 2097152
  47.8 1.3 %copy.17 = f32[256,2048]{1,0:T(8,128)} copy(f32[256,2048]{1,0:T(8,128)S(1)} %get-tuple-element.4) | data formatting | bytes 4194304

commit v2 on v1

--- a/solution.py
+++ b/solution.py
@@ -592,6 +592,7 @@
     kzr,
     kfin,
     fin,
+    bulk,
     in_sem,
     send_sem,
     recv_sem,
@@ -622,9 +623,11 @@
     def sem(*key):
         return keys.setdefault(key, len(keys))
 
-    def fetch(src_ref, dst_ref):
-        copy = pltpu.make_async_copy(src_ref, dst_ref, in_sem.at[counts["in"]])
-        counts["in"] += 1
+    def fetch(src_ref, dst_ref, at=None):
+        if at is None:
+            at = counts["in"]
+            counts["in"] += 1
+        copy = pltpu.make_async_copy(src_ref, dst_ref, in_sem.at[at])
         copy.start()
         return copy
 
@@ -661,20 +664,24 @@
     got_o.wait()
     pl.semaphore_wait(barrier, nT - 1 + nS - 1)
 
-    pending = []
+    pending, sent = [], []
 
     def remote(src_ref, dst_ref, key, where, keep=True):
+        shared = keep and src_ref.dtype == BF16
+        if shared:
+            sent.append(math.prod(src_ref.shape) * 2)
         copy = pltpu.make_async_remote_copy(
             src_ref=src_ref,
             dst_ref=dst_ref,
-            send_sem=send_sem.at[len(pending)],
+            send_sem=send_sem.at[0 if shared else len(pending) + 1],
             recv_sem=recv_sem.at[sem(*key) if isinstance(key, tuple) else key],
             device_id=where,
             device_id_type=pl.DeviceIdType.MESH,
         )
         if keep:
             copy.start()
-        pending.append((copy, keep))
+        if not shared:
+            pending.append((copy, keep))
         return copy
 
     def arrive(dst_ref, key, where):
@@ -960,7 +967,6 @@
         with scope(f"w_{kind}s"):
             arrive(kvbuf.at[1, 2 * chip + other], (kind, "s"), sib)
 
-    remote(kvown.at[x], kvbuf.at[1, t], ("ke",), to_peer)
     remote(kvown.at[ox], kvpeer, ("kp",), to_peer)
     with scope("w_ns"):
         arrive(nbuf.at[x, other], ("n", "s"), sib)
@@ -971,41 +977,42 @@
     got_w.wait()
     got_saved.wait()
     project_o(0)
+    remote(kvown.at[x], kvbuf.at[1, t], ("ke",), to_peer)
     with scope("w_kvs"):
         arrive(kvbuf.at[0, x * 2 + other], ("kv", "s"), sib)
     attend(0, 0, 0, 0)
     pass_on(nbuf, "n")
-    peer_keys(x, "ke")
     passed(nbuf, "n")
     project_q(1)
-    peer_keys_end(x, "ke")
-    attend(0, 0, 1, 0)
-    pass_on(obuf, "o")
     with scope("w_kpx"):
         arrive(kvpeer, ("kp",), to_peer)
     remote(kvpeer, kvbuf.at[1, t], ("kx",), across)
+    pass_on(obuf, "o")
     passed(obuf, "o")
     project_o(1)
     slice_sends()
     attend(0, 1, 0, 0)
-    attend(0, 1, 1, 0)
+    need(0)
+    attend(1, 0, 0, 0)
     with scope("w_kvx"):
         arrive(kvbuf.at[0, 2 * ox + c], ("kv", "x"), across)
     remote(kvbuf.at[0, 2 * ox + c], kvbuf.at[0, 2 * ox + c], ("kv", "t"), sib)
-    need(0)
-    attend(1, 0, 0, 0)
-    attend(1, 0, 1, 0)
+    peer_keys(x, "ke")
     with scope("w_kvt"):
         arrive(kvbuf.at[0, 2 * ox + other], ("kv", "t"), sib)
+    attend(0, 0, 0, 1)
     attend(1, 0, 0, 1)
-    attend(0, 0, 0, 1)
     peer_keys(ox, "kx")
     attend(0, 1, 0, 1)
+    peer_keys_end(x, "ke")
+    attend(1, 0, 1, 0)
     peer_keys_end(ox, "kx")
     attend(1, 0, 1, 1)
     grad_out(1, 0)
+    attend(0, 0, 1, 0)
     attend(0, 0, 1, 1)
     grad_out(0, 0)
+    attend(0, 1, 1, 0)
     attend(0, 1, 1, 1)
     need(1)
     attend(1, 1, 1, 0)
@@ -1043,6 +1050,8 @@
     weight_piece(3)
 
     with scope("w_send"):
+        whole = bulk.at[pl.ds(0, sum(sent) // (bulk.shape[1] * 4))]
+        pltpu.make_async_copy(whole, whole, send_sem.at[0]).wait()
         for copy, kept in pending:
             if kept:
                 copy.wait_send()
@@ -1092,9 +1101,10 @@
         vm((2, sr, kv), BF16),
         vm((2, sr, kv), BF16),
         vm((2, sr, kv), BF16),
+        vm((8 * sr, width // 2), F32),
         pltpu.SemaphoreType.DMA((12,)),
-        pltpu.SemaphoreType.DMA((74,)),
-        pltpu.SemaphoreType.DMA((80,)),
+        pltpu.SemaphoreType.DMA((6,)),
+        pltpu.SemaphoreType.DMA((48,)),
     ]
 
 

time: 49.3 us -> 47.7 us (0.968); the launches traced: 49.1 us -> 47 us
  Pallas kernels: 45.5 us -> 43.4 us
    pallas_call x1, Pallas kernels: 45.5 us -> 43.4 us  [shards(): pl.pallas_call(body, out_shape=(pltpu.VMEM((nr, width), F32), pltpu.VMEM(...]
where the time goes in v2:
time: 47.7 us; the launch traced here: 47 us
  Pallas kernels  43.4 us (91%)
  local copies, waits for them, and re-layouts  2.99 us (6%)
  between operations  0.64 us (1%)
    pallas_call x1, Pallas kernels, shards(): pl.pallas_call(body, out_shape=(pltpu.VMEM((nr, width), F32), pltpu.VMEM(...  43.4 us
    unnamed x3, local copies, waits for them, and re-layouts  2.99 us

profile of v2, /device:TPU:1, one launch (start us, length us, event | category | flops | bytes accessed | tf_op | source)
XLA Modules:
  0.0 47.0 jit_solution(4218026997520093203)
XLA Ops:
  0.6 43.4 %cross_back.1 = (f32[32,2048]{1,0:T(8,128)S(1)}, f32[256,2048]{1,0:T(8,128)S(1)}, f32[512,512]{1,0:T(8,128)S(1)}) custom-call(bf16[32,2048]{1,0:T(8,128)(2,1)} %target.1, bf16[256,2048]{1,0:T(8,128)(2,1)} %source.1, f32[1,2048]{1,0:T(1,128)} %bitcast.1, bf16[2048,512]{1,0:T(8,128)(2,1)} %query_weight.1, bf16[2048,256]{1,0:T(8,128)(2,1)} %key_weight.1, ...), custom_call_target="tpu_custom_call" | custom-call | tf_op jit(solution)/shard_map/cross_back/pallas_call | solution.py:1182
  44.0 0.7 %copy.16 = f32[32,2048]{1,0:T(8,128)} copy(f32[32,2048]{1,0:T(8,128)S(1)} %get-tuple-element.3) | data formatting | bytes 524288
  44.7 1.0 %copy.18 = f32[512,512]{1,0:T(8,128)} copy(f32[512,512]{1,0:T(8,128)S(1)} %get-tuple-element.5) | data formatting | bytes 2097152
  45.7 1.3 %copy.17 = f32[256,2048]{1,0:T(8,128)} copy(f32[256,2048]{1,0:T(8,128)S(1)} %get-tuple-element.4) | data formatting | bytes 4194304

commit v3 on v2

--- a/solution.py
+++ b/solution.py
@@ -631,6 +631,16 @@
         copy.start()
         return copy
 
+    barrier = pltpu.get_barrier_semaphore()
+    for k in range(1, nT):
+        pl.semaphore_signal(
+            barrier, 1, device_id={"tp": (t + k) % nT}, device_id_type=pl.DeviceIdType.MESH
+        )
+    for k in range(1, nS):
+        pl.semaphore_signal(
+            barrier, 1, device_id={"sp": (s + k) % nS}, device_id_type=pl.DeviceIdType.MESH
+        )
+
     got_t = fetch(target, tgt)
     got_g = fetch(norm_gain, gain)
     got_shift = fetch(log_shift, shift)
@@ -645,16 +655,6 @@
     got_q = fetch(query_weight, wq)
     got_w = fetch(output_weight, wo)
     got_saved = fetch(saved_out, saved)
-
-    barrier = pltpu.get_barrier_semaphore()
-    for k in range(1, nT):
-        pl.semaphore_signal(
-            barrier, 1, device_id={"tp": (t + k) % nT}, device_id_type=pl.DeviceIdType.MESH
-        )
-    for k in range(1, nS):
-        pl.semaphore_signal(
-            barrier, 1, device_id={"sp": (s + k) % nS}, device_id_type=pl.DeviceIdType.MESH
-        )
 
     got_t.wait()
     got_g.wait()
@@ -701,6 +701,12 @@
     remote(nbuf.at[x, c], nbuf.at[x, c], ("n", "s"), sib)
     remote(obuf.at[x, c], obuf.at[x, c], ("o", "s"), sib)
     remote(obuf.at[x, c], obuf.at[x, c], ("o", "x"), across)
+    def slice_sends():
+        for v, where, to in ((2, to_peer, peer), (1, to_far, far), (3, to_diag, diag)):
+            cols = pl.ds(pl.multiple_of(to * ds_width, HEAD_DIM), ds_width)
+            remote(nbuf.at[x, c, :, cols], nall.at[v, x, c], ("na", v), where)
+
+    slice_sends()
     for copy in got_kv:
         copy.wait()
     with scope("kvproj"):
@@ -818,11 +824,6 @@
                 kz[i] = key_sum(1, i).astype(BF16)
         remote(kz, kzr, ("kz",), to_peer)
 
-    def slice_sends():
-        for v, where, to in ((2, to_peer, peer), (1, to_far, far), (3, to_diag, diag)):
-            cols = pl.ds(pl.multiple_of(to * ds_width, HEAD_DIM), ds_width)
-            remote(nbuf.at[x, c, :, cols], nall.at[v, x, c], ("na", v), where)
-
     def slice_from(v):
         return (None, to_far, to_peer, to_diag)[v]
 
@@ -984,30 +985,29 @@
     pass_on(nbuf, "n")
     passed(nbuf, "n")
     project_q(1)
+    pass_on(obuf, "o")
     with scope("w_kpx"):
         arrive(kvpeer, ("kp",), to_peer)
     remote(kvpeer, kvbuf.at[1, t], ("kx",), across)
-    pass_on(obuf, "o")
     passed(obuf, "o")
     project_o(1)
-    slice_sends()
+    with scope("w_kvx"):
+        arrive(kvbuf.at[0, 2 * ox + c], ("kv", "x"), across)
+    remote(kvbuf.at[0, 2 * ox + c], kvbuf.at[0, 2 * ox + c], ("kv", "t"), sib)
     attend(0, 1, 0, 0)
     need(0)
     attend(1, 0, 0, 0)
-    with scope("w_kvx"):
-        arrive(kvbuf.at[0, 2 * ox + c], ("kv", "x"), across)
-    remote(kvbuf.at[0, 2 * ox + c], kvbuf.at[0, 2 * ox + c], ("kv", "t"), sib)
-    peer_keys(x, "ke")
     with scope("w_kvt"):
         arrive(kvbuf.at[0, 2 * ox + other], ("kv", "t"), sib)
     attend(0, 0, 0, 1)
     attend(1, 0, 0, 1)
     peer_keys(ox, "kx")
     attend(0, 1, 0, 1)
+    peer_keys(x, "ke")
+    peer_keys_end(ox, "kx")
+    attend(1, 0, 1, 1)
     peer_keys_end(x, "ke")
     attend(1, 0, 1, 0)
-    peer_keys_end(ox, "kx")
-    attend(1, 0, 1, 1)
     grad_out(1, 0)
     attend(0, 0, 1, 0)
     attend(0, 0, 1, 1)
@@ -1021,9 +1021,9 @@
     attend(1, 1, 0, 0)
     attend(1, 1, 0, 1)
     grad_out(1, 1)
+    grad_out(0, 1)
     send_keys(0)
     keys_back()
-    grad_out(0, 1)
     for v in (1, 2, 3):
         slice_pass(v)
     nall[0] = nbuf[:, :, :, pl.ds(pl.multiple_of(s * ds_width, HEAD_DIM), ds_width)]

time: 47.7 us -> 47.1 us (0.987); the launches traced: 47 us -> 46.9 us
  no operation moved by 1% of the time
where the time goes in v3:
time: 47.1 us; the launch traced here: 46.9 us
  Pallas kernels  43.3 us (92%)
  local copies, waits for them, and re-layouts  2.99 us (6%)
  between operations  0.64 us (1%)
    pallas_call x1, Pallas kernels, shards(): pl.pallas_call(body, out_shape=(pltpu.VMEM((nr, width), F32), pltpu.VMEM(...  43.3 us
    unnamed x3, local copies, waits for them, and re-layouts  2.99 us

profile of v3, /device:TPU:1, one launch (start us, length us, event | category | flops | bytes accessed | tf_op | source)
XLA Modules:
  0.0 46.9 jit_solution(3407327407840111564)
XLA Ops:
  0.6 43.3 %cross_back.1 = (f32[32,2048]{1,0:T(8,128)S(1)}, f32[256,2048]{1,0:T(8,128)S(1)}, f32[512,512]{1,0:T(8,128)S(1)}) custom-call(bf16[32,2048]{1,0:T(8,128)(2,1)} %target.1, bf16[256,2048]{1,0:T(8,128)(2,1)} %source.1, f32[1,2048]{1,0:T(1,128)} %bitcast.1, bf16[2048,512]{1,0:T(8,128)(2,1)} %query_weight.1, bf16[2048,256]{1,0:T(8,128)(2,1)} %key_weight.1, ...), custom_call_target="tpu_custom_call" | custom-call | tf_op jit(solution)/shard_map/cross_back/pallas_call | solution.py:1182
  43.9 0.7 %copy.16 = f32[32,2048]{1,0:T(8,128)} copy(f32[32,2048]{1,0:T(8,128)S(1)} %get-tuple-element.3) | data formatting | bytes 524288
  44.6 1.0 %copy.18 = f32[512,512]{1,0:T(8,128)} copy(f32[512,512]{1,0:T(8,128)S(1)} %get-tuple-element.5) | data formatting | bytes 2097152
  45.6 1.3 %copy.17 = f32[256,2048]{1,0:T(8,128)} copy(f32[256,2048]{1,0:T(8,128)S(1)} %get-tuple-element.4) | data formatting | bytes 4194304

commit v4 on v3

--- a/solution.py
+++ b/solution.py
@@ -771,10 +771,14 @@
 
     def attend(v, k, a, g):
         with scope(f"attend_{v}{k}{a}{g}"):
-            attend_rows(v, k, a, g)
-
-    def attend_rows(v, k, a, g):
-        pair = pl.ds(2 * (x if g == 0 else ox), 2)
+            attend_rows(v, k, a, g, x if g == 0 else ox)
+
+    def attend_last(a, mine):
+        with scope(f"last_{a}{mine}"):
+            attend_rows(1, 1, a, 2, c if mine else other)
+
+    def attend_rows(v, k, a, g, chip):
+        pair = pl.ds(2 * chip, 2)
         sr = kvbuf.shape[2]
         k_rows = kvbuf[a, pair, :, :HEAD_DIM].reshape(2 * sr, HEAD_DIM)
         v_rows = kvbuf[a, pair, :, HEAD_DIM:].reshape(2 * sr, HEAD_DIM)
@@ -787,7 +791,7 @@
         value_part = jnp.dot(prob.astype(BF16), backs, preferred_element_type=F32)
         key_part = key_part.reshape(2, sr, HEAD_DIM)
         value_part = value_part.reshape(2, sr, HEAD_DIM)
-        if (a, g) not in got["kacc"]:
+        if g < 2 and (a, g) not in got["kacc"]:
             kacc[a, pair, :, :HEAD_DIM] = key_part
             kacc[a, pair, :, HEAD_DIM:] = value_part
         else:
@@ -1015,15 +1019,15 @@
     attend(0, 1, 1, 0)
     attend(0, 1, 1, 1)
     need(1)
-    attend(1, 1, 1, 0)
-    attend(1, 1, 1, 1)
+    attend_last(1, 0)
     send_keys(1)
-    attend(1, 1, 0, 0)
-    attend(1, 1, 0, 1)
+    attend_last(1, 1)
+    attend_last(0, 0)
+    send_keys(0)
+    attend_last(0, 1)
     grad_out(1, 1)
+    keys_back()
     grad_out(0, 1)
-    send_keys(0)
-    keys_back()
     for v in (1, 2, 3):
         slice_pass(v)
     nall[0] = nbuf[:, :, :, pl.ds(pl.multiple_of(s * ds_width, HEAD_DIM), ds_width)]

time: 47.1 us -> 46.2 us (0.981)
  Pallas kernels: 43.3 us -> 42.5 us
    pallas_call x1, Pallas kernels: 43.3 us -> 42.5 us  [shards(): pl.pallas_call(body, out_shape=(pltpu.VMEM((nr, width), F32), pltpu.VMEM(...]
where the time goes in v4:
time: 46.2 us; the launch traced here: 46.1 us
  Pallas kernels  42.5 us (92%)
  local copies, waits for them, and re-layouts  2.99 us (6%)
  between operations  0.64 us (1%)
    pallas_call x1, Pallas kernels, shards(): pl.pallas_call(body, out_shape=(pltpu.VMEM((nr, width), F32), pltpu.VMEM(...  42.5 us
    unnamed x3, local copies, waits for them, and re-layouts  2.99 us

profile of v4, /device:TPU:1, one launch (start us, length us, event | category | flops | bytes accessed | tf_op | source)
XLA Modules:
  0.0 46.1 jit_solution(10409211744918954555)
XLA Ops:
  0.6 42.5 %cross_back.1 = (f32[32,2048]{1,0:T(8,128)S(1)}, f32[256,2048]{1,0:T(8,128)S(1)}, f32[512,512]{1,0:T(8,128)S(1)}) custom-call(bf16[32,2048]{1,0:T(8,128)(2,1)} %target.1, bf16[256,2048]{1,0:T(8,128)(2,1)} %source.1, f32[1,2048]{1,0:T(1,128)} %bitcast.1, bf16[2048,512]{1,0:T(8,128)(2,1)} %query_weight.1, bf16[2048,256]{1,0:T(8,128)(2,1)} %key_weight.1, ...), custom_call_target="tpu_custom_call" | custom-call | tf_op jit(solution)/shard_map/cross_back/pallas_call | solution.py:1186
  43.1 0.7 %copy.16 = f32[32,2048]{1,0:T(8,128)} copy(f32[32,2048]{1,0:T(8,128)S(1)} %get-tuple-element.3) | data formatting | bytes 524288
  43.8 1.0 %copy.18 = f32[512,512]{1,0:T(8,128)} copy(f32[512,512]{1,0:T(8,128)S(1)} %get-tuple-element.5) | data formatting | bytes 2097152
  44.8 1.3 %copy.17 = f32[256,2048]{1,0:T(8,128)} copy(f32[256,2048]{1,0:T(8,128)S(1)} %get-tuple-element.4) | data formatting | bytes 4194304

commit v5 on v4

--- a/solution.py
+++ b/solution.py
@@ -1024,9 +1024,20 @@
     attend_last(1, 1)
     attend_last(0, 0)
     send_keys(0)
+    ends = (s == 0) | (s == nS - 1)
+
+    @pl.when(jnp.logical_not(ends))
+    def _():
+        keys_back()
+
     attend_last(0, 1)
     grad_out(1, 1)
-    keys_back()
+
+    @pl.when(ends)
+    def _():
+        keys_back()
+
+    sent.pop()
     grad_out(0, 1)
     for v in (1, 2, 3):
         slice_pass(v)

time: 46.2 us -> 46.1 us (level)
  no operation moved by 1% of the time
where the time goes in v5:
time: 46.1 us; the launch traced here: 46 us
  Pallas kernels  42.3 us (92%)
  local copies, waits for them, and re-layouts  2.99 us (6%)
  between operations  0.64 us (1%)
    pallas_call x1, Pallas kernels, shards(): pl.pallas_call(body, out_shape=(pltpu.VMEM((nr, width), F32), pltpu.VMEM(...  42.3 us
    unnamed x3, local copies, waits for them, and re-layouts  2.99 us

profile of v5, /device:TPU:1, one launch (start us, length us, event | category | flops | bytes accessed | tf_op | source)
XLA Modules:
  0.0 46.0 jit_solution(13130843575849279890)
XLA Ops:
  0.6 42.3 %cross_back.1 = (f32[32,2048]{1,0:T(8,128)S(1)}, f32[256,2048]{1,0:T(8,128)S(1)}, f32[512,512]{1,0:T(8,128)S(1)}) custom-call(bf16[32,2048]{1,0:T(8,128)(2,1)} %target.1, bf16[256,2048]{1,0:T(8,128)(2,1)} %source.1, f32[1,2048]{1,0:T(1,128)} %bitcast.1, bf16[2048,512]{1,0:T(8,128)(2,1)} %query_weight.1, bf16[2048,256]{1,0:T(8,128)(2,1)} %key_weight.1, ...), custom_call_target="tpu_custom_call" | custom-call | tf_op jit(solution)/shard_map/cross_back/pallas_call | solution.py:1197
  43.0 0.7 %copy.16 = f32[32,2048]{1,0:T(8,128)} copy(f32[32,2048]{1,0:T(8,128)S(1)} %get-tuple-element.3) | data formatting | bytes 524288
  43.7 1.0 %copy.18 = f32[512,512]{1,0:T(8,128)} copy(f32[512,512]{1,0:T(8,128)S(1)} %get-tuple-element.5) | data formatting | bytes 2097152
  44.6 1.3 %copy.17 = f32[256,2048]{1,0:T(8,128)} copy(f32[256,2048]{1,0:T(8,128)S(1)} %get-tuple-element.4) | data formatting | bytes 4194304
